TPU v7x, 32 devices: a whole 2x2x4 slice. The times are simulated.
32 devices in a mesh: ep: 16 (over z, y, x), tp: 2 (over core).
Axes of the slice: x: 2, y: 2, z: 4, core: 2. Of those that a mesh axis runs over, the one named last changes fastest.
Arguments:
- tokens: bfloat16 [4096, 1024], P('ep'), may hold values from -6 to 6
- norm_gain: float32 [1024], replicated, may hold values from 0.1 to 1.9
- routing: int32 [4096, 2], P('ep'), may hold values from 0 to 31, all different within a row; in each aligned block of 256 rows (0 to 255, 256 to 511, ...) at most 16 rows name the same one
- route_weights: float32 [4096, 2], P('ep'), may hold values from 0.1 to 1
- lengths: int32 [1024], P('ep'), may hold values from 1 to 4, 2560 in all
- w_gate: bfloat16 [32, 1024, 3584], P('ep', None, 'tp'), may hold values from -0.1875 to 0.1875
- w_up: bfloat16 [32, 1024, 3584], P('ep', None, 'tp'), may hold values from -0.1875 to 0.1875
- w_down: bfloat16 [32, 3584, 1024], P('ep', 'tp'), may hold values from -0.09375 to 0.09375
Outputs:
- mixed: bfloat16 [4096, 1024], P('ep', 'tp')
Inputs may be any that keep to these rules, and one draw needn't show every extreme that they name: `routing`: each row names 2 different experts; at most 16 rows of one device name the same expert, and that many is reached.
All inputs are finite; a program needn't handle non-finite values. No bound on the sum of `lengths` on one device may be relied on, other than what follows from the above.
Results may differ from a plain program's by a relative error of at most 0.009.
Values may be sent and summed in bfloat16 or wider, within the bound.
A program may use at most 64 MiB of HBM per device.

v0:
```python
import jax
import jax.numpy as jnp
from jax import lax
from jax.sharding import PartitionSpec as P

SPAN = 4


eps = 1e-06


def per_device(tokens, norm_gain, routing, route_weights, lengths, w_gate, w_up, w_down):
    ep_count = lax.axis_size("ep")
    local_experts = w_gate.shape[0]
    experts_all = ep_count * local_experts
    tok_rows = tokens.shape[0]
    model_width = tokens.shape[1]
    chosen = routing.shape[1]
    bound = 2 * ((tok_rows * chosen + 2 * experts_all - 1) // (2 * experts_all))
    slots_all = experts_all * bound
    floats = tokens.astype(jnp.float32)
    normed = (
        floats * lax.rsqrt(jnp.mean(floats * floats, axis=-1, keepdims=True) + eps) * norm_gain
    ).astype(jnp.bfloat16)
    position = jnp.arange(tok_rows, dtype=jnp.int32)
    live_rows = position % SPAN < jnp.repeat(lengths, SPAN)
    expert_ids = routing.reshape(-1)
    live_picks = jnp.repeat(live_rows, chosen)
    onehot = (
        (expert_ids[:, None] == jnp.arange(experts_all, dtype=jnp.int32)[None, :])
        & live_picks[:, None]
    ).astype(jnp.int32)
    before = jnp.cumsum(onehot, axis=0) - onehot
    slot_rank = jnp.sum(before * onehot, axis=1)
    slot_index = jnp.where(live_picks, expert_ids * bound + slot_rank, slots_all)
    picked = (slot_index[None, :] == jnp.arange(slots_all, dtype=jnp.int32)[:, None]).reshape(
        slots_all, tok_rows, chosen
    )
    placing = jnp.any(picked, axis=2).astype(jnp.bfloat16)
    outgoing = jnp.dot(placing, normed, preferred_element_type=jnp.float32).astype(jnp.bfloat16)
    outgoing = outgoing.reshape(ep_count, local_experts, bound, model_width)
    incoming = lax.all_to_all(outgoing, "ep", split_axis=0, concat_axis=0, tiled=True)
    gate_proj = jnp.einsum("sxcd,xdf->sxcf", incoming, w_gate, preferred_element_type=jnp.float32)
    up_proj = jnp.einsum("sxcd,xdf->sxcf", incoming, w_up, preferred_element_type=jnp.float32)
    hidden = (jax.nn.silu(gate_proj) * up_proj).astype(jnp.bfloat16)
    partial_out = jnp.einsum("sxcf,xfd->sxcd", hidden, w_down, preferred_element_type=jnp.float32)
    expert_out = lax.psum_scatter(
        partial_out.astype(jnp.bfloat16), "tp", scatter_dimension=3, tiled=True
    )
    returned = lax.all_to_all(expert_out, "ep", split_axis=0, concat_axis=0, tiled=True)
    returned = returned.reshape(slots_all, returned.shape[3])
    combine = jnp.sum(jnp.where(picked, route_weights[None, :, :], 0.0), axis=2)
    mixed = jnp.einsum(
        "st,sd->td", combine, returned.astype(jnp.float32), precision=lax.Precision.HIGHEST
    )
    return mixed.astype(jnp.bfloat16)


def solution(mesh):
    placed = (
        P("ep", None),
        P(),
        P("ep", None),
        P("ep", None),
        P("ep"),
        P("ep", None, "tp"),
        P("ep", None, "tp"),
        P("ep", "tp", None),
    )
    return jax.shard_map(
        per_device, mesh=mesh, in_specs=placed, out_specs=P("ep", "tp"), check_vma=False
    )
```

profile of v0, /device:TPU:0, one launch (start us, length us, event | category | flops | bytes accessed | tf_op | source)
XLA Modules:
  0.0 107.5 jit_solution(11050893328938252070)
XLA Ops:
  6.5 0.0 reduce-scatter.2.cloned.1.call-start
  6.5 0.8 copy.38
  7.4 0.1 eq.45
  7.5 0.1 eq.41
  7.6 0.7 broadcast_in_dim.40
  8.4 0.1 broadcast_in_dim.41
  8.5 0.1 broadcast_in_dim.42
  8.6 0.1 broadcast_in_dim.43
  8.7 0.2 broadcast_in_dim.44
  8.9 1.2 %reduce-window.6 = s32[32,4,128]{2,0,1:T(8,128)S(1)} reduce-window(s32[32,4,128]{2,0,1:T(8,128)S(1)} %fusion.40, s32[]{:T(128)} %constant.29.clone.1), window={size=1x1x128 pad=0_0x0_0x127_0}, to_apply=%region_0.0 | reduce-window | flops 2080768 | bytes 131076 | tf_op jit(solution)/shard_map/reduce-window
  10.0 0.2 slice_reduce_fusion
  10.3 0.7 broadcast_in_dim.38
  11.0 0.1 reshape.71
  11.1 0.1 broadcast_in_dim.39.clone
  11.3 0.2 and.26
  11.4 0.1 fusion.37
  11.5 0.1 reduce_sum.30
  11.7 0.1 copy.42
  11.7 0.7 add_select_fusion.1
  12.4 0.2 fusion.28
  12.6 1.2 %fusion.25 = f32[256]{0:T(256)S(1)} fusion(bf16[256,1024]{1,0:T(8,128)(2,1)} %param.8), kind=kLoop, calls=%fused_computation.20 | loop fusion | flops 786176 | bytes 525312 | tf_op jit(solution)/shard_map/reduce_sum | solution.py:23
  13.9 1.6 %convolution_convert_fusion = bf16[512,1024]{1,0:T(8,128)(2,1)S(1)} fusion(pred[512,256]{1,0:T(8,128)(4,1)S(1)} %fusion.28, bf16[256,1024]{1,0:T(8,128)(2,1)} %param.8, f32[1024]{0:T(1024)} %param.9, f32[256]{0:T(256)S(1)} %add_rsqrt_fusion), kind=kOutput, calls=%fused_computation.15 | convolution fusion | flops 270008320 | bytes 1709056 | tf_op jit(solution)/shard_map/dot_general | solution.py:40
  15.5 34.5 %all_to_all.10 = bf16[16,2,16,1024]{3,2,1,0:T(8,128)(2,1)S(1)} all-to-all(bf16[16,2,16,1024]{3,2,1,0:T(8,128)(2,1)S(1)} %bitcast.83), channel_id=1, replica_groups=mesh['ep'=16,'tp'=2] {'ep'}, dimensions={0} | all-to-all | bytes 2097152 | tf_op jit(solution)/shard_map/all_to_all | solution.py:42
  49.9 7.0 %fusion.4 = f32[2,16,16,1792]{3,2,1,0:T(8,128)} fusion(bf16[2,1024,1792]{2,1,0:T(8,128)(2,1)} %param.13, bf16[16,2,16,1024]{3,2,1,0:T(8,128)(2,1)S(1)} %all_to_all.10), kind=kOutput, calls=%fused_computation.4 | convolution fusion | flops 1879048192 | bytes 12058624 | tf_op jit(solution)/shard_map/sxcd,xdf->sxcf/dot_general | solution.py:43
  56.9 11.3 %fusion.20 = bf16[16,2,16,1024]{3,2,0,1:T(8,128)(2,1)} fusion(bf16[2,1792,1024]{2,1,0:T(8,128)(2,1)} %param.15, f32[2,16,16,1792]{3,2,1,0:T(8,128)} %fusion.4, bf16[2,1024,1792]{2,1,0:T(8,128)(2,1)} %param.14, bf16[16,2,16,1024]{3,2,1,0:T(8,128)(2,1)S(1)} %all_to_all.10), kind=kOutput, calls=%fused_computation.16 | convolution fusion | flops 3764125696 | bytes 20447232 | tf_op jit(solution)/shard_map/sxcf,xfd->sxcd/dot_general | solution.py:46
  68.2 0.0 reduce-scatter.2.cloned.1.call-update
  68.2 6.9 %reduce-scatter.2.cloned.1.call-done = bf16[16,2,16,512]{3,2,0,1:T(8,128)(2,1)} async-done(((bf16[16,2,16,1024]{3,2,0,1:T(8,128)(2,1)}), bf16[16,2,16,512]{3,2,0,1:T(8,128)(2,1)}) %reduce-scatter.2.cloned.1.call-update) | async-done | bytes 524304 | tf_op jit(solution)/shard_map/reduce_scatter | solution.py:47
  75.1 1.9 %copy.45 = bf16[16,2,16,512]{3,2,1,0:T(8,128)(2,1)} copy(bf16[16,2,16,512]{3,2,0,1:T(8,128)(2,1)} %reduce-scatter.2.cloned.1.call-done) | data formatting | bytes 1048576 | tf_op jit(solution)/shard_map/reduce_scatter | solution.py:47
  77.0 6.8 %all-to-all-start.1 = ((bf16[16,2,16,512]{3,2,1,0:T(8,128)(2,1)}), bf16[16,2,16,512]{3,2,1,0:T(8,128)(2,1)S(1)}, u32[]{:S(2)}, u32[]{:S(2)}) async-start(bf16[16,2,16,512]{3,2,1,0:T(8,128)(2,1)} %copy.45), calls=%async_computation.2 | async-start | bytes 1048576 | tf_op jit(solution)/shard_map/all_to_all | solution.py:50
  83.8 0.2 select_reduce_fusion
  84.0 15.3 %all-to-all-done.1 = bf16[16,2,16,512]{3,2,1,0:T(8,128)(2,1)S(1)} async-done(((bf16[16,2,16,512]{3,2,1,0:T(8,128)(2,1)}), bf16[16,2,16,512]{3,2,1,0:T(8,128)(2,1)S(1)}, u32[]{:S(2)}, u32[]{:S(2)}) %all-to-all-start.1) | async-done | bytes 524320 | tf_op jit(solution)/shard_map/all_to_all | solution.py:50
  99.3 1.3 %convolution_convert_fusion.1 = bf16[256,512]{1,0:T(8,128)(2,1)} fusion(f32[512,256]{1,0:T(8,128)S(1)} %select_reduce_fusion, bf16[512,512]{1,0:T(8,128)(2,1)S(1)} %bitcast.82), kind=kOutput, calls=%fused_computation.19 | convolution fusion | flops 805437440 | bytes 1310720 | tf_op jit(solution)/shard_map/st,sd->td/dot_general | solution.py:53
  (8 shorter events, 0.1 us)
Async XLA Ops:
  6.5 68.6 %reduce-scatter.2.cloned.1.call-start = ((), (), s32[]{:S(2)}) async-start(), calls=%async_computation.3 | async-start | bytes 1572864 | tf_op jit(solution)/shard_map/reduce_scatter | solution.py:47
  56.9 26.9 %copy-start = (f32[256,2]{0,1:T(2,128)S(1)}, f32[256,2]{0,1:T(2,128)}, u32[]{:S(2)}) copy-start(f32[256,2]{0,1:T(2,128)} %param.11) | copy-start | bytes 6148
  77.0 22.3 %all-to-all-start.1 = ((bf16[16,2,16,512]{3,2,1,0:T(8,128)(2,1)}), bf16[16,2,16,512]{3,2,1,0:T(8,128)(2,1)S(1)}, u32[]{:S(2)}, u32[]{:S(2)}) async-start(bf16[16,2,16,512]{3,2,1,0:T(8,128)(2,1)} %copy.45), calls=%async_computation.2 | async-start | bytes 1048576 | tf_op jit(solution)/shard_map/all_to_all | solution.py:50
Sparse Core Ops, SparseCore 0:
  68.4 6.7 reduce-scatter.1
where the time goes:
time: 108 us; the launch traced here: 107 us
  blocking collectives  34.5 us (32%)
  waiting for transfers between devices  22.2 us (21%)
  matrix products  21.2 us (20%)
  between operations  13.5 us (12%)
  starting transfers between devices  6.78 us (6%)
  local copies, waits for them, and re-layouts  5.69 us (5%)
  other arithmetic  3.65 us (3%)
    all_to_all x1, blocking collectives, per_device(): lax.all_to_all(outgoing, 'ep', split_axis=0, concat_axis=0, tiled=True)  34.5 us
    all_to_all x1, waiting for transfers between devices, per_device(): lax.all_to_all(expert_out, 'ep', split_axis=0, concat_axis=0, tiled=True)  15.3 us
    dot_general x1, matrix products, per_device(): jnp.einsum('sxcf,xfd->sxcd', hidden, w_down, preferred_element_type=jnp.f...  11.3 us
    dot_general x1, matrix products, per_device(): jnp.einsum('sxcd,xdf->sxcf', incoming, w_gate, preferred_element_type=jnp...  6.97 us
    reduce_scatter x1, waiting for transfers between devices, per_device(): lax.psum_scatter(partial_out.astype(jnp.bfloat16), 'tp', scatter_dimensio...  6.87 us
    all_to_all x1, starting transfers between devices, per_device(): lax.all_to_all(expert_out, 'ep', split_axis=0, concat_axis=0, tiled=True)  6.77 us
  transfers between devices with their start and end apart: 2, of which 2 were waited for; matrix products, arithmetic and copies ran while one was open for 0% of the time, Pallas kernels for 0%

commit v1 on v0

v1 whole, which is shorter than its diff:
```python
import functools

import jax
import jax.numpy as jnp
from jax import lax
from jax.experimental import pallas as pl
from jax.experimental.pallas import tpu as pltpu
from jax.sharding import PartitionSpec as P

MESH = pl.DeviceIdType.MESH
GROUPS = 2
TILE = 16
eps = 1e-06
BF = jnp.bfloat16
F32 = jnp.float32


def dot(a, b):
    return jnp.dot(a, b, preferred_element_type=F32)


def kernel(
    n, groups, local, bound, span,
    gain_ref, routing_ref, weights_ref, lengths_ref,
    tokens_hbm, gate_hbm, up_hbm, down_hbm,
    out_ref,
    tok, gate_w, up_w, down_w, outgoing, incoming, hidden, partial, theirs, returning, returned, comb,
    tok_sem, w_sem, disp_send, disp_recv, fwd_send, fwd_recv, part_send, part_recv, ret_send, ret_recv,
):
    me = lax.axis_index("ep")
    core = lax.axis_index("tp")
    other = 1 - core
    pow2 = n & (n - 1) == 0
    per = n // groups
    rows = per * bound
    group_slots = local * rows
    tok_rows, width = tok.shape
    half = width // 2
    chosen = routing_ref.shape[0]
    experts = n * local
    mine = pl.ds(pl.multiple_of(core * half, half), half)

    def target(k):
        return lax.bitwise_xor(me, k) if pow2 else lax.rem(me + k, n)

    barrier = pltpu.get_barrier_semaphore()
    for k in range(1, n):
        pl.semaphore_signal(barrier, inc=1, device_id=(target(k), core), device_id_type=MESH)
    pl.semaphore_signal(barrier, inc=1, device_id=(me, other), device_id_type=MESH)

    tok_copy = pltpu.make_async_copy(tokens_hbm, tok, tok_sem)
    tok_copy.start()
    loads = {}
    for x in range(local):
        for i, (src, dst) in enumerate(((gate_hbm, gate_w), (up_hbm, up_w), (down_hbm, down_w))):
            loads[x, i] = pltpu.make_async_copy(src.at[x], dst.at[x], w_sem.at[x, i])
            loads[x, i].start()

    count = lengths_ref.shape[1]
    spread = (
        lax.broadcasted_iota(jnp.int32, (count, tok_rows), 1) // span
        == lax.broadcasted_iota(jnp.int32, (count, tok_rows), 0)
    ).astype(BF)
    lens = jnp.broadcast_to(lengths_ref[...].astype(F32), (8, count)).astype(BF)
    live_len = dot(lens, spread)[0:1]
    place = lax.broadcasted_iota(jnp.int32, (1, tok_rows), 1) % span
    live = place.astype(F32) < live_len
    routing = routing_ref[...]
    ids = lax.broadcasted_iota(jnp.int32, (experts, tok_rows), 0)
    named = ids == routing[0:1]
    for i in range(1, chosen):
        named = named | (ids == routing[i : i + 1])
    named = named & live
    earlier = (
        lax.broadcasted_iota(jnp.int32, (tok_rows, tok_rows), 0)
        < lax.broadcasted_iota(jnp.int32, (tok_rows, tok_rows), 1)
    ).astype(BF)
    rank = dot(jnp.where(named, 1.0, 0.0).astype(BF), earlier)
    rank = jnp.where(named, rank, -1.0).astype(BF)

    def slot_ids(shape, g):
        s = lax.broadcasted_iota(jnp.int32, shape, 0)
        k = (s // bound) % per * groups + g
        peer = lax.bitwise_xor(jnp.full(shape, me, jnp.int32), k) if pow2 else (me + k) % n
        return peer * local + s // rows, s % bound

    tok_copy.wait()
    floats = tok[...].astype(F32)
    scale = lax.rsqrt(jnp.mean(floats * floats, axis=-1, keepdims=True) + eps)
    normed = (tok[:, mine].astype(F32) * scale * gain_ref[:, mine]).astype(BF)

    def dispatch(k):
        g, j = k % groups, k // groups
        return pltpu.make_async_remote_copy(
            src_ref=outgoing.at[g, :, j],
            dst_ref=incoming.at[g, :, j, :, mine],
            send_sem=disp_send.at[k],
            recv_sem=disp_recv.at[k],
            device_id=(target(k), core),
            device_id_type=MESH,
        )

    def forward(k):
        g, j = k % groups, k // groups
        return pltpu.make_async_remote_copy(
            src_ref=incoming.at[g, :, j, :, mine],
            dst_ref=incoming.at[g, :, j, :, mine],
            send_sem=fwd_send.at[k],
            recv_sem=fwd_recv.at[k],
            device_id=(me, other),
            device_id_type=MESH,
        )

    def swap(g, x):
        return pltpu.make_async_remote_copy(
            src_ref=partial.at[g, x, other],
            dst_ref=theirs.at[g, x],
            send_sem=part_send.at[g, x],
            recv_sem=part_recv.at[g, x],
            device_id=(me, other),
            device_id_type=MESH,
        )

    def give_back(k, x):
        g, j = k % groups, k // groups
        return pltpu.make_async_remote_copy(
            src_ref=returning.at[g, x, j],
            dst_ref=returned.at[g, x, j],
            send_sem=ret_send.at[k, x],
            recv_sem=ret_recv.at[k, x],
            device_id=(target((n - k) % n if not pow2 else k), core),
            device_id_type=MESH,
        )

    def members(g):
        return list(range(g, n, groups))

    for g in range(groups):
        owner, slot = slot_ids((group_slots, experts), g)
        to_expert = (owner == lax.broadcasted_iota(jnp.int32, (group_slots, experts), 1)).astype(BF)
        owner, slot = slot_ids((group_slots, tok_rows), g)
        hit = dot(to_expert, rank) == slot.astype(F32)
        block = dot(jnp.where(hit, 1.0, 0.0).astype(BF), normed).astype(BF)
        block = block.reshape(local, per, bound, half)
        outgoing[g] = block
        if g == 0:
            incoming[0, :, 0, :, mine] = block[:, 0]
            pl.semaphore_wait(barrier, n)
        for k in reversed(members(g)):
            if k:
                dispatch(k).start()
        if g == 0:
            forward(0).start()
    for g in range(groups):
        owner, slot = slot_ids((group_slots, experts), g)
        to_expert = (owner == lax.broadcasted_iota(jnp.int32, (group_slots, experts), 1)).astype(BF)
        owner, slot = slot_ids((group_slots, tok_rows), g)
        hit = dot(to_expert, rank) == slot.astype(F32)
        value = jnp.zeros((group_slots, tok_rows), F32)
        for i in range(chosen):
            value = jnp.where(owner == routing[i : i + 1], weights_ref[i : i + 1], value)
        comb[g] = jnp.where(hit, value, 0.0).T

    def arrive(g):
        for k in members(g):
            if k:
                dispatch(k).wait_recv()
                forward(k).start()

    arrive(0)
    for g in range(groups):
        for k in members(g):
            forward(k).wait_recv()
        for x in range(local):
            xs = incoming[g, x].reshape(rows, width)
            if g == 0:
                loads[x, 0].wait()
            gate = dot(xs, gate_w[x])
            if g == 0:
                loads[x, 1].wait()
            hidden[...] = (gate / (1.0 + jnp.exp(-gate)) * dot(xs, up_w[x])).astype(BF)
            if g == 0:
                loads[x, 2].wait()
            down = dot(hidden[...], down_w[x]).astype(BF)
            partial[g, x, 0] = down[:, :half]
            partial[g, x, 1] = down[:, half:]
            swap(g, x).start()
        if g + 1 < groups:
            arrive(g + 1)
        for x in range(local):
            swap(g, x).wait_recv()
            total = (partial[g, x, core].astype(F32) + theirs[g, x].astype(F32)).astype(BF)
            total = total.reshape(per, bound, half)
            returning[g, x] = total
            if g == 0:
                returned[0, x, 0] = total[0]
            for k in reversed(members(g)):
                if k:
                    give_back(k, x).start()
    mixed = jnp.zeros((tok_rows, half), F32)
    for g in range(groups):
        for x in range(local):
            for k in members(g):
                if k:
                    give_back(k, x).wait_recv()
        values = returned[g].reshape(group_slots, half)
        weight = comb[g]
        high = weight.astype(BF)
        low = (weight - high.astype(F32)).astype(BF)
        mixed = mixed + dot(high, values) + dot(low, values)
    out_ref[...] = mixed.astype(BF)
    for k in range(n):
        if k:
            dispatch(k).wait_send()
            for x in range(local):
                give_back(k, x).wait_send()
        forward(k).wait_send()
    for g in range(groups):
        for x in range(local):
            swap(g, x).wait_send()


def per_device(n, tokens, norm_gain, routing, route_weights, lengths, w_gate, w_up, w_down):
    local, width, units = w_gate.shape
    tok_rows, chosen = routing.shape
    experts = n * local
    groups = GROUPS
    bound = 2 * ((tok_rows * chosen + 2 * experts - 1) // (2 * experts))
    bound = (bound + TILE - 1) // TILE * TILE
    half = width // 2
    per = n // groups
    rows = per * bound
    span = tok_rows // lengths.shape[0]
    vmem = pl.BlockSpec(memory_space=pltpu.VMEM)
    hbm = pl.BlockSpec(memory_space=pl.ANY)
    dma = pltpu.SemaphoreType.DMA
    return pl.pallas_call(
        functools.partial(kernel, n, groups, local, bound, span),
        out_shape=jax.ShapeDtypeStruct((tok_rows, half), BF),
        in_specs=[vmem] * 4 + [hbm] * 4,
        out_specs=vmem,
        scratch_shapes=[
            pltpu.VMEM((tok_rows, width), BF),
            pltpu.VMEM((local, width, units), BF),
            pltpu.VMEM((local, width, units), BF),
            pltpu.VMEM((local, units, width), BF),
            pltpu.VMEM((groups, local, per, bound, half), BF),
            pltpu.VMEM((groups, local, per, bound, width), BF),
            pltpu.VMEM((rows, units), BF),
            pltpu.VMEM((groups, local, 2, rows, half), BF),
            pltpu.VMEM((groups, local, rows, half), BF),
            pltpu.VMEM((groups, local, per, bound, half), BF),
            pltpu.VMEM((groups, local, per, bound, half), BF),
            pltpu.VMEM((groups, tok_rows, local * rows), F32),
            dma,
            dma((local, 3)),
            dma((n,)),
            dma((n,)),
            dma((n,)),
            dma((n,)),
            dma((groups, local)),
            dma((groups, local)),
            dma((n, local)),
            dma((n, local)),
        ],
        compiler_params=pltpu.CompilerParams(
            collective_id=0, has_side_effects=True, vmem_limit_bytes=63 * 1024 * 1024
        ),
    )(
        norm_gain.reshape(1, width),
        routing.T,
        route_weights.T,
        lengths.reshape(1, -1),
        tokens,
        w_gate,
        w_up,
        w_down,
    )


def solution(mesh):
    placed = (
        P("ep", None),
        P(),
        P("ep", None),
        P("ep", None),
        P("ep"),
        P("ep", None, "tp"),
        P("ep", None, "tp"),
        P("ep", "tp", None),
    )
    return jax.shard_map(
        functools.partial(per_device, mesh.shape["ep"]),
        mesh=mesh, in_specs=placed, out_specs=P("ep", "tp"), check_vma=False,
    )
```

time: 108 us -> 43 us (0.40)
  Pallas kernels: 0 us -> 41.1 us
  blocking collectives: 34.5 us -> 0 us
  waiting for transfers between devices: 22.2 us -> 0 us
  matrix products: 21.2 us -> 0 us
  between operations: 13.5 us -> 0.01 us
  starting transfers between devices: 6.78 us -> 0 us
  local copies, waits for them, and re-layouts: 5.69 us -> 1.67 us
  other arithmetic: 3.65 us -> 0 us
    pallas_call x0 -> x1, Pallas kernels: none -> 41.1 us  [per_device(): pl.pallas_call(functools.partial(kernel, n, groups, local, bound, span),...]
    all_to_all x1 -> x0, blocking collectives: 34.5 us -> none  [per_device(): lax.all_to_all(outgoing, 'ep', split_axis=0, concat_axis=0, tiled=True)]
    dot_general x4 -> x0, matrix products: 21.2 us -> none  [the longest x1 11.3 us: per_device(): jnp.einsum('sxcf,xfd->sxcd', hidden, w_down, preferred_element_type=jnp.f...]
    all_to_all x1 -> x0, waiting for transfers between devices: 15.3 us -> none  [per_device(): lax.all_to_all(expert_out, 'ep', split_axis=0, concat_axis=0, tiled=True)]
    reduce_scatter x1 -> x0, waiting for transfers between devices: 6.87 us -> none  [per_device(): lax.psum_scatter(partial_out.astype(jnp.bfloat16), 'tp', scatter_dimensio...]
    all_to_all x1 -> x0, starting transfers between devices: 6.77 us -> none  [per_device(): lax.all_to_all(expert_out, 'ep', split_axis=0, concat_axis=0, tiled=True)]
    broadcast_in_dim x7 -> x0, local copies, waits for them, and re-layouts: 2 us -> none  [the longest x4 1.64 us: per_device(): live_rows = position % SPAN < jnp.repeat(lengths, SPAN)]
    reduce_scatter x1 -> x0, local copies, waits for them, and re-layouts: 1.89 us -> none  [per_device(): lax.psum_scatter(partial_out.astype(jnp.bfloat16), 'tp', scatter_dimensio...]
  transfers between devices with their start and end apart: 2 -> 0, of which waited for: 2 -> 0; matrix products, arithmetic and copies ran while one was open for 0% -> 0% of each run, Pallas kernels for 0% -> 0%
where the time goes in v1:
time: 43 us; the launch traced here: 42.8 us
  Pallas kernels  41.1 us (96%)
  local copies, waits for them, and re-layouts  1.67 us (4%)
    pallas_call x1, Pallas kernels, per_device(): pl.pallas_call(functools.partial(kernel, n, groups, local, bound, span),...  41.1 us
    unnamed x1, local copies, waits for them, and re-layouts  1.67 us

profile of v1, /device:TPU:0, one launch (start us, length us, event | category | flops | bytes accessed | tf_op | source)
XLA Modules:
  0.0 42.8 jit_solution(13011861970237663238)
XLA Ops:
  0.0 41.1 %shard_map.82 = bf16[256,512]{1,0:T(8,128)(2,1)} custom-call(f32[1,1024]{1,0:T(1,128)} %bitcast.4, s32[2,256]{1,0:T(2,128)} %bitcast.5, f32[2,256]{1,0:T(2,128)} %bitcast.6, s32[1,64]{1,0:T(1,128)} %bitcast.7, bf16[256,1024]{1,0:T(8,128)(2,1)} %tokens_hbm.1, bf16[2,1024,1792]{2,1,0:T(8,128)(2,1)} %gate_hbm.1, bf16[2,1024,1792]{2,1,0:T(8,128)(2,1)} %up_hbm.1, ...), custom_call_target="tpu_custom_call" | custom-call | tf_op jit(solution)/shard_map/pallas_call | solution.py:237
  41.1 1.7 %copy.10 = bf16[256,512]{1,0:T(8,128)(2,1)} copy(bf16[256,512]{1,0:T(8,128)(2,1)} %shard_map.82) | data formatting | bytes 524288

commit v2 on v1

--- a/solution.py
+++ b/solution.py
@@ -21,11 +21,11 @@
 
 def kernel(
     n, groups, local, bound, span,
-    gain_ref, routing_ref, weights_ref, lengths_ref,
+    gain_hbm, routing_hbm, weights_hbm, lengths_hbm,
     tokens_hbm, gate_hbm, up_hbm, down_hbm,
     out_ref,
-    tok, gate_w, up_w, down_w, outgoing, incoming, hidden, partial, theirs, returning, returned, comb,
-    tok_sem, w_sem, disp_send, disp_recv, fwd_send, fwd_recv, part_send, part_recv, ret_send, ret_recv,
+    gain_ref, routing_ref, weights_ref, lengths_ref, tok, gate_w, up_w, down_w, outgoing, incoming, hidden, partial, theirs, returning, returned, comb,
+    small_sem, tok_sem, w_sem, disp_send, disp_recv, fwd_send, fwd_recv, part_send, part_recv, ret_send, ret_recv,
 ):
     me = lax.axis_index("ep")
     core = lax.axis_index("tp")
@@ -43,18 +43,33 @@
     def target(k):
         return lax.bitwise_xor(me, k) if pow2 else lax.rem(me + k, n)
 
+    small = [
+        pltpu.make_async_copy(src, dst, small_sem.at[i])
+        for i, (src, dst) in enumerate((
+            (lengths_hbm, lengths_ref),
+            (routing_hbm, routing_ref),
+            (gain_hbm, gain_ref),
+            (weights_hbm, weights_ref),
+        ))
+    ]
+    tok_copy = pltpu.make_async_copy(tokens_hbm, tok, tok_sem)
+    tok_copy.start()
+    for copy in small:
+        copy.start()
+
     barrier = pltpu.get_barrier_semaphore()
     for k in range(1, n):
         pl.semaphore_signal(barrier, inc=1, device_id=(target(k), core), device_id_type=MESH)
     pl.semaphore_signal(barrier, inc=1, device_id=(me, other), device_id_type=MESH)
 
-    tok_copy = pltpu.make_async_copy(tokens_hbm, tok, tok_sem)
-    tok_copy.start()
     loads = {}
     for x in range(local):
         for i, (src, dst) in enumerate(((gate_hbm, gate_w), (up_hbm, up_w), (down_hbm, down_w))):
             loads[x, i] = pltpu.make_async_copy(src.at[x], dst.at[x], w_sem.at[x, i])
             loads[x, i].start()
+
+    for copy in small:
+        copy.wait()
 
     count = lengths_ref.shape[1]
     spread = (
@@ -135,7 +150,7 @@
     def members(g):
         return list(range(g, n, groups))
 
-    for g in range(groups):
+    def fill(g):
         owner, slot = slot_ids((group_slots, experts), g)
         to_expert = (owner == lax.broadcasted_iota(jnp.int32, (group_slots, experts), 1)).astype(BF)
         owner, slot = slot_ids((group_slots, tok_rows), g)
@@ -145,12 +160,19 @@
         outgoing[g] = block
         if g == 0:
             incoming[0, :, 0, :, mine] = block[:, 0]
-            pl.semaphore_wait(barrier, n)
+
+    def send(g):
         for k in reversed(members(g)):
             if k:
                 dispatch(k).start()
-        if g == 0:
-            forward(0).start()
+
+    fill(0)
+    pl.semaphore_wait(barrier, n)
+    send(0)
+    forward(0).start()
+    for g in range(1, groups):
+        fill(g)
+        send(g)
     for g in range(groups):
         owner, slot = slot_ids((group_slots, experts), g)
         to_expert = (owner == lax.broadcasted_iota(jnp.int32, (group_slots, experts), 1)).astype(BF)
@@ -166,6 +188,17 @@
             if k:
                 dispatch(k).wait_recv()
                 forward(k).start()
+
+    def finish(g, x):
+        swap(g, x).wait_recv()
+        total = (partial[g, x, core].astype(F32) + theirs[g, x].astype(F32)).astype(BF)
+        total = total.reshape(per, bound, half)
+        returning[g, x] = total
+        if g == 0:
+            returned[0, x, 0] = total[0]
+        for k in reversed(members(g)):
+            if k:
+                give_back(k, x).start()
 
     arrive(0)
     for g in range(groups):
@@ -181,22 +214,15 @@
             hidden[...] = (gate / (1.0 + jnp.exp(-gate)) * dot(xs, up_w[x])).astype(BF)
             if g == 0:
                 loads[x, 2].wait()
+            if x:
+                finish(g, x - 1)
             down = dot(hidden[...], down_w[x]).astype(BF)
             partial[g, x, 0] = down[:, :half]
             partial[g, x, 1] = down[:, half:]
             swap(g, x).start()
         if g + 1 < groups:
             arrive(g + 1)
-        for x in range(local):
-            swap(g, x).wait_recv()
-            total = (partial[g, x, core].astype(F32) + theirs[g, x].astype(F32)).astype(BF)
-            total = total.reshape(per, bound, half)
-            returning[g, x] = total
-            if g == 0:
-                returned[0, x, 0] = total[0]
-            for k in reversed(members(g)):
-                if k:
-                    give_back(k, x).start()
+        finish(g, local - 1)
     mixed = jnp.zeros((tok_rows, half), F32)
     for g in range(groups):
         for x in range(local):
@@ -232,14 +258,18 @@
     rows = per * bound
     span = tok_rows // lengths.shape[0]
     vmem = pl.BlockSpec(memory_space=pltpu.VMEM)
-    hbm = pl.BlockSpec(memory_space=pl.ANY)
+    hbm = pl.BlockSpec(memory_space=pltpu.HBM)
     dma = pltpu.SemaphoreType.DMA
     return pl.pallas_call(
         functools.partial(kernel, n, groups, local, bound, span),
-        out_shape=jax.ShapeDtypeStruct((tok_rows, half), BF),
-        in_specs=[vmem] * 4 + [hbm] * 4,
+        out_shape=pltpu.VMEM((tok_rows, half), BF),
+        in_specs=[hbm] * 8,
         out_specs=vmem,
         scratch_shapes=[
+            pltpu.VMEM((1, width), F32),
+            pltpu.VMEM((chosen, tok_rows), jnp.int32),
+            pltpu.VMEM((chosen, tok_rows), F32),
+            pltpu.VMEM((1, lengths.shape[0]), jnp.int32),
             pltpu.VMEM((tok_rows, width), BF),
             pltpu.VMEM((local, width, units), BF),
             pltpu.VMEM((local, width, units), BF),
@@ -252,6 +282,7 @@
             pltpu.VMEM((groups, local, per, bound, half), BF),
             pltpu.VMEM((groups, local, per, bound, half), BF),
             pltpu.VMEM((groups, tok_rows, local * rows), F32),
+            dma((4,)),
             dma,
             dma((local, 3)),
             dma((n,)),
@@ -264,7 +295,7 @@
             dma((n, local)),
         ],
         compiler_params=pltpu.CompilerParams(
-            collective_id=0, has_side_effects=True, vmem_limit_bytes=63 * 1024 * 1024
+            collective_id=0, has_side_effects=True, vmem_limit_bytes=66000000
         ),
     )(
         norm_gain.reshape(1, width),

time: 43 us -> 36.6 us (0.85)
  Pallas kernels: 41.1 us -> 35.8 us
  local copies, waits for them, and re-layouts: 1.67 us -> 0.71 us
    pallas_call x1, Pallas kernels: 41.1 us -> 35.8 us  [per_device(): pl.pallas_call(functools.partial(kernel, n, groups, local, bound, span),...]
    unnamed x1, local copies, waits for them, and re-layouts: 1.67 us -> 0.71 us
where the time goes in v2:
time: 36.6 us; the launch traced here: 36.5 us
  Pallas kernels  35.8 us (98%)
  local copies, waits for them, and re-layouts  0.71 us (2%)
    pallas_call x1, Pallas kernels, per_device(): pl.pallas_call(functools.partial(kernel, n, groups, local, bound, span),...  35.8 us

profile of v2, /device:TPU:0, one launch (start us, length us, event | category | flops | bytes accessed | tf_op | source)
XLA Modules:
  0.0 36.5 jit_solution(1054721138045430106)
XLA Ops:
  0.0 35.8 %shard_map.82 = bf16[256,512]{1,0:T(8,128)(2,1)S(1)} custom-call(f32[1,1024]{1,0:T(1,128)} %bitcast.4, s32[2,256]{1,0:T(2,128)} %bitcast.5, f32[2,256]{1,0:T(2,128)} %bitcast.6, s32[1,64]{1,0:T(1,128)} %bitcast.7, bf16[256,1024]{1,0:T(8,128)(2,1)} %tokens_hbm.1, bf16[2,1024,1792]{2,1,0:T(8,128)(2,1)} %gate_hbm.1, bf16[2,1024,1792]{2,1,0:T(8,128)(2,1)} %up_hbm.1, ...), custom_call_target="tpu_custom_call" | custom-call | tf_op jit(solution)/shard_map/pallas_call | solution.py:263
  35.8 0.7 %copy.10 = bf16[256,512]{1,0:T(8,128)(2,1)} copy(bf16[256,512]{1,0:T(8,128)(2,1)S(1)} %shard_map.82) | data formatting | bytes 524288
